TPU v7x, 32 devices: a whole 2x2x4 slice. The times are simulated.
32 devices in a mesh: sp: 4 (over y, x), tp: 8 (over z, core).
Axes of the slice: x: 2, y: 2, z: 4, core: 2. Of those that a mesh axis runs over, the one named last changes fastest.
Arguments:
- layer_input: bfloat16 [2048, 2048], P(('sp', 'tp')), may hold values from -6 to 6
- receptance: bfloat16 [2048, 2048], P('sp', 'tp'), may hold values from -6 to 6
- keys: bfloat16 [2048, 2048], P('sp', 'tp'), may hold values from -6 to 6
- values: bfloat16 [2048, 2048], P('sp', 'tp'), may hold values from -6 to 6
- erase_preact: bfloat16 [2048, 2048], P('sp', 'tp'), may hold values from -12 to 5
- decay_preact: bfloat16 [2048, 2048], P('sp', 'tp'), may hold values from -40 to 3
- decay_spike: float32 [2048, 32], P('sp', 'tp'), may hold values from -2 to 0
- head_norm_gain: bfloat16 [2048], P('tp'), may hold values from 0.099609375 to 1.8984375
- output_weight: bfloat16 [2048, 2048], P('tp'), may hold values from -0.125 to 0.125
- expert_norm_gain: bfloat16 [2048], replicated, may hold values from 0.099609375 to 1.8984375
- routes: int32 [2048, 2], P(('sp', 'tp')), may hold values from 0 to 7, all different within a row; in each aligned block of 64 rows (0 to 63, 64 to 127, ...) at most 24 rows name the same one
- routing_weight: float32 [2048, 2], P(('sp', 'tp')), may hold values from 0.3 to 1.5
- expert_gate_weight: bfloat16 [8, 2048, 4096], P('sp', None, 'tp'), may hold values from -0.125 to 0.125
- expert_up_weight: bfloat16 [8, 2048, 4096], P('sp', None, 'tp'), may hold values from -0.125 to 0.125
- expert_down_weight: bfloat16 [8, 4096, 2048], P('sp', 'tp'), may hold values from -0.09375 to 0.09375
- shared_gate_weight: bfloat16 [2048, 4096], P(None, 'tp'), may hold values from -0.125 to 0.125
- shared_up_weight: bfloat16 [2048, 4096], P(None, 'tp'), may hold values from -0.125 to 0.125
- shared_down_weight: bfloat16 [4096, 2048], P('tp'), may hold values from -0.09375 to 0.09375
Outputs:
- layer_out: bfloat16 [2048, 2048], P(('sp', 'tp'))
Inputs may be any that keep to these rules, and one draw needn't show every extreme that they name: `routes`: in each aligned block of 64 rows no expert is named by more than 24 rows.
All inputs are finite; a program needn't handle non-finite values.
Results may differ from a plain program's by a relative error of at most 0.02.
Values may be sent and summed in bfloat16 or wider, within the bound.
No kernel may reach another device: no remote copies, remote signals or barrier semaphores. Data moves between devices by JAX's collectives and lax.ppermute only.
A program may use at most 128 MiB of HBM per device.

v0:
```python
import jax
import jax.numpy as jnp
from jax import lax
from jax.sharding import PartitionSpec as P

BLOCK = 64


highest = lax.Precision.HIGHEST
GN_EPS = 0.00064
RMS_EPS = 1e-06


def entering(array, axis, combine, identity, reverse):
    size, place = (lax.axis_size(axis), lax.axis_index(axis))
    everything = jax.tree.map(
        lambda part, kind: lax.all_gather(part.astype(kind), axis),
        array,
        (jnp.bfloat16, jnp.bfloat16),
    )
    start = jax.tree.map(
        lambda part, zero: jnp.broadcast_to(jnp.asarray(zero, part.dtype), part.shape),
        array,
        identity,
    )

    def step(k, before):
        at = size - 1 - k if reverse else k
        reached = at > place if reverse else at < place
        new = combine(
            before, jax.tree.map(lambda part, own: part[at].astype(own.dtype), everything, array)
        )
        return jax.tree.map(lambda a, b: jnp.where(reached, a, b), new, before)

    return lax.fori_loop(0, size, step, start)


def chain_product(left_mat, right_mat):
    return jnp.einsum("...ij,...jk->...ik", left_mat, right_mat, precision=highest)


def compose(earlier, later):
    return (chain_product(earlier[0], later[0]), chain_product(earlier[1], later[0]) + later[1])


def block_terms(decay_logarithm, unit_keys, beta, key_rows, value_rows, read_rows, span_len):
    tokens_here, head_number, head_width = key_rows.shape
    block_count = tokens_here // span_len

    def to_blocks(array):
        return jnp.swapaxes(array.reshape(block_count, span_len, head_number, head_width), 1, 2)

    decay_logarithm, unit_keys, beta, key_rows, value_rows, read_rows = [
        to_blocks(array)
        for array in (decay_logarithm, unit_keys, beta, key_rows, value_rows, read_rows)
    ]
    cumulative = jnp.cumsum(decay_logarithm, axis=2)
    ending = cumulative[:, :, -1:, :]
    unit_scaled = unit_keys * jnp.exp(cumulative - decay_logarithm)
    read_scaled = read_rows * jnp.exp(cumulative)
    beta_scaled = beta * jnp.exp(-cumulative)
    key_scaled = key_rows * jnp.exp(-cumulative)
    row_ids = lax.broadcasted_iota(jnp.int32, (span_len, span_len), 0)
    col_ids = lax.broadcasted_iota(jnp.int32, (span_len, span_len), 1)

    def pairs(left_rows, right_rows, keep):
        return jnp.where(
            keep, jnp.einsum("bhtn,bhsn->bhts", left_rows, right_rows, precision=highest), 0.0
        )

    def apply_rows(weights, rows_in):
        return jnp.einsum("bhts,bhsn->bhtn", weights, rows_in, precision=highest)

    erase_beta = pairs(unit_scaled, beta_scaled, row_ids > col_ids)
    erase_key = pairs(unit_scaled, key_scaled, row_ids > col_ids)
    read_beta = pairs(read_scaled, beta_scaled, row_ids >= col_ids)
    read_key = pairs(read_scaled, key_scaled, row_ids >= col_ids)
    triangle = erase_beta + (row_ids == col_ids).astype(jnp.float32)
    right_side = jnp.concatenate([unit_scaled, -apply_rows(erase_key, value_rows)], axis=-1)
    solved = jax.scipy.linalg.solve_triangular(triangle, right_side, lower=True, unit_diagonal=True)
    lead_rows = solved[..., :head_width]
    own_rows = solved[..., head_width:]
    local = apply_rows(read_beta, own_rows) + apply_rows(read_key, value_rows)
    readout = read_scaled - apply_rows(read_beta, lead_rows)
    beta_end = beta * jnp.exp(ending - cumulative)
    key_end = key_rows * jnp.exp(ending - cumulative)
    diagonal = jnp.exp(ending)[:, :, 0, :, None] * jnp.eye(head_width, dtype=jnp.float32)
    transition = diagonal - jnp.einsum("bhtn,bhtm->bhnm", lead_rows, beta_end, precision=highest)
    carried = jnp.einsum("bhtv,bhtm->bhvm", own_rows, beta_end, precision=highest) + jnp.einsum(
        "bhtv,bhtm->bhvm", value_rows, key_end, precision=highest
    )
    return (local, readout, transition, carried)


def block_chain(transition, carried):
    head_number, head_width = (transition.shape[1], transition.shape[2])
    identity = jnp.broadcast_to(
        jnp.eye(head_width, dtype=jnp.float32), (head_number, head_width, head_width)
    )

    def advance(running, block_pair):
        product, state_now = running
        updated = (
            chain_product(product, block_pair[0]),
            chain_product(state_now, block_pair[0]) + block_pair[1],
        )
        return (updated, (product, state_now))

    (whole_map, ending), (prefix, starts) = lax.scan(
        advance, (identity, jnp.zeros_like(identity)), (transition, carried)
    )
    return (whole_map, ending, prefix, starts)


def sweep(arrays, span_len):
    local, readout, transition, carried = block_terms(*arrays, span_len)
    whole_map, ending, prefix, starts = block_chain(transition, carried)
    return ((local, readout, prefix, starts), (whole_map, ending))


def finish(parts, entry):
    local, readout, prefix, starts = parts
    start_state = jnp.einsum("hvn,bhnm->bhvm", entry, prefix, precision=highest) + starts
    result = local + jnp.einsum("bhtn,bhvn->bhtv", readout, start_state, precision=highest)
    return jnp.swapaxes(result, 1, 2).reshape(-1, result.shape[1], result.shape[3])


def body(
    layer_input,
    receptance,
    keys,
    values,
    erase_preact,
    decay_preact,
    decay_spike,
    head_norm_gain,
    output_weight,
    expert_norm_gain,
    routes,
    routing_weight,
    expert_gate_weight,
    expert_up_weight,
    expert_down_weight,
    shared_gate_weight,
    shared_up_weight,
    shared_down_weight,
):
    tokens_here = keys.shape[0]
    head_number = decay_spike.shape[1]
    head_width = keys.shape[1] // head_number

    def each_head(array):
        return array.astype(jnp.float32).reshape(tokens_here, head_number, head_width)

    key_rows = each_head(keys)
    unit_keys = key_rows * lax.rsqrt(jnp.sum(key_rows * key_rows, axis=-1, keepdims=True) + 1e-06)
    beta = unit_keys * jax.nn.sigmoid(each_head(erase_preact))
    decay_logarithm = (
        -jnp.exp(-jax.nn.softplus(-each_head(decay_preact)) - 0.5) + decay_spike[:, :, None]
    )
    arrays = (decay_logarithm, unit_keys, beta, key_rows, each_head(values), each_head(receptance))
    forward_parts, forward_map = sweep(arrays, BLOCK)
    backward_parts, backward_map = sweep(tuple((array[::-1] for array in arrays)), BLOCK)
    identity = jnp.broadcast_to(jnp.eye(head_width, dtype=jnp.float32), forward_map[0].shape)
    blank = jnp.zeros_like(forward_map[1])
    forward_entry = entering(
        (forward_map[0], forward_map[1]), "sp", compose, (identity, blank), False
    )[1]
    backward_entry = entering(
        (backward_map[0], backward_map[1]), "sp", compose, (identity, blank), True
    )[1]
    mix = finish(forward_parts, forward_entry) + finish(backward_parts, backward_entry)[::-1]
    center = jnp.mean(mix, axis=-1, keepdims=True)
    spread = jnp.mean(jnp.square(mix - center), axis=-1, keepdims=True)
    mixed = ((mix - center) * lax.rsqrt(spread + GN_EPS)).reshape(
        tokens_here, head_number * head_width
    )
    mixed = (mixed * head_norm_gain.astype(jnp.float32)).astype(jnp.bfloat16)
    row_count = layer_input.shape[0]
    model_width = layer_input.shape[1]
    slab = mixed
    projected = lax.psum_scatter(
        jnp.dot(slab, output_weight, preferred_element_type=jnp.float32).astype(jnp.bfloat16),
        "tp",
        scatter_dimension=0,
        tiled=True,
    ).astype(jnp.float32)
    residual = layer_input.astype(jnp.float32) + projected
    normed = residual * lax.rsqrt(jnp.mean(residual * residual, axis=-1, keepdims=True) + RMS_EPS)
    normed = (normed * expert_norm_gain.astype(jnp.float32)).astype(jnp.bfloat16)
    top_count = routes.shape[1]
    expert_local = expert_gate_weight.shape[0]
    sp_count = lax.axis_size("sp")
    expert_total = expert_local * sp_count
    capacity = max(2, (3 * row_count * top_count + 2 * expert_total - 1) // (2 * expert_total))
    slot_total = sp_count * capacity * expert_local
    entries = routes.reshape(-1)
    entry_count = entries.shape[0]
    expert_hot = (entries[:, None] == lax.broadcasted_iota(jnp.int32, (1, expert_total), 1)).astype(
        jnp.int32
    )
    rank_in = jnp.sum((jnp.cumsum(expert_hot, axis=0) - 1) * expert_hot, axis=1)
    slot_of = (entries // expert_local * capacity + rank_in) * expert_local + entries % expert_local
    slot_hot = (slot_of[:, None] == lax.broadcasted_iota(jnp.int32, (1, slot_total), 1)).astype(
        jnp.float32
    )
    owner_hot = (
        lax.broadcasted_iota(jnp.int32, (entry_count, 1), 0) // top_count
        == lax.broadcasted_iota(jnp.int32, (1, row_count), 1)
    ).astype(jnp.float32)
    placing = jnp.dot(slot_hot.T, owner_hot, precision=highest)
    weighting = jnp.dot(owner_hot.T, slot_hot * routing_weight.reshape(-1, 1), precision=highest)
    outgoing = jnp.dot(placing.astype(jnp.bfloat16), normed, preferred_element_type=jnp.float32)
    outgoing = outgoing.astype(jnp.bfloat16).reshape(sp_count, capacity, expert_local, model_width)
    arrived = lax.all_to_all(outgoing, "sp", split_axis=0, concat_axis=0, tiled=True)
    own_block = jnp.concatenate([arrived.reshape(slot_total, model_width), normed], axis=0)
    block_rows = own_block.shape[0]
    everyone = lax.all_gather(own_block, "tp", axis=0, tiled=True)
    slab = everyone
    slab = slab.reshape(block_rows * lax.axis_size("tp") // block_rows, block_rows, model_width)
    routed_in = slab[:, :slot_total].reshape(-1, expert_local, model_width)
    gate_value = jnp.einsum(
        "rjd,jdh->rjh", routed_in, expert_gate_weight, preferred_element_type=jnp.float32
    )
    up_value = jnp.einsum(
        "rjd,jdh->rjh", routed_in, expert_up_weight, preferred_element_type=jnp.float32
    )
    hidden = (jax.nn.silu(gate_value) * up_value).astype(jnp.bfloat16)
    routed_out = jnp.einsum(
        "rjh,jhd->rjd", hidden, expert_down_weight, preferred_element_type=jnp.float32
    )
    routed_out = routed_out.reshape(-1, slot_total, model_width)
    shared_in = slab[:, slot_total:].reshape(-1, model_width)
    shared_hidden = (
        jax.nn.silu(jnp.dot(shared_in, shared_gate_weight, preferred_element_type=jnp.float32))
        * jnp.dot(shared_in, shared_up_weight, preferred_element_type=jnp.float32)
    ).astype(jnp.bfloat16)
    shared_out = jnp.dot(shared_hidden, shared_down_weight, preferred_element_type=jnp.float32)
    shared_out = shared_out.reshape(-1, row_count, model_width)
    summed = lax.psum_scatter(
        jnp.concatenate([routed_out, shared_out], axis=1)
        .reshape(block_rows * lax.axis_size("tp"), model_width)
        .astype(jnp.bfloat16),
        "tp",
        scatter_dimension=0,
        tiled=True,
    ).astype(jnp.float32)
    routed_rows = (
        summed[:slot_total]
        .astype(jnp.bfloat16)
        .reshape(sp_count, capacity, expert_local, model_width)
    )
    returned = lax.all_to_all(routed_rows, "sp", split_axis=0, concat_axis=0, tiled=True)
    routed = jnp.dot(
        weighting, returned.reshape(slot_total, model_width).astype(jnp.float32), precision=highest
    )
    return (residual + summed[slot_total:] + routed).astype(jnp.bfloat16)


def solution(mesh):
    return jax.shard_map(
        body,
        mesh=mesh,
        in_specs=(
            P(("sp", "tp"), None),
            P("sp", "tp"),
            P("sp", "tp"),
            P("sp", "tp"),
            P("sp", "tp"),
            P("sp", "tp"),
            P("sp", "tp"),
            P("tp"),
            P("tp", None),
            P(),
            P(("sp", "tp"), None),
            P(("sp", "tp"), None),
            P("sp", None, "tp"),
            P("sp", None, "tp"),
            P("sp", "tp", None),
            P(None, "tp"),
            P(None, "tp"),
            P("tp", None),
        ),
        out_specs=P(("sp", "tp"), None),
        check_vma=False,
    )
```

profile of v0, /device:TPU:0, one launch (start us, length us, event | category | flops | bytes accessed | tf_op | source)
XLA Modules:
  0.0 987.2 jit_solution(1634263152878162815)
XLA Ops:
  36.5 5.8 convolution_select_fusion.4
  58.8 159.2 %custom-call.8 = f32[8,4,1,64,64]{3,4,2,1,0:T(8,128)} custom-call(f32[8,4,1,64,64]{4,3,2,1,0:T(8,128)} %fusion.66), custom_call_target="InvertDiagBlocksLowerTriangular" | custom-call | tf_op jit(solution)/shard_map/jit(_solve_triangular)/vmap(vmap())/triangular_solve | solution.py:80
  305.0 158.7 %custom-call.9 = f32[8,4,1,64,64]{3,4,2,1,0:T(8,128)} custom-call(f32[8,4,1,64,64]{4,3,2,1,0:T(8,128)} %fusion.62), custom_call_target="InvertDiagBlocksLowerTriangular" | custom-call | tf_op jit(solution)/shard_map/jit(_solve_triangular)/vmap(vmap())/triangular_solve | solution.py:80
  483.9 35.3 %while.64 = (s32[]{:T(128)}, f32[4,64,64]{1,2,0:T(8,128)S(1)}, f32[4,64,64]{1,2,0:T(8,128)S(1)}, f32[8,4,64,64]{2,3,1,0:T(8,128)}, f32[8,4,64,64]{2,3,1,0:T(8,12...) while((s32[]{:T(128)}, f32[4,64,64]{1,2,0:T(8,128)S(1)}, ...), condition=%wide.region_3.5_spmd.clone, body=%wide.region_2.4_spmd.clone.sunk | while | flops 25214980 | bytes 1507456 | solution.py:109
  519.4 11.5 %all-gather = bf16[16,64,64]{2,1,0:T(8,128)(2,1)} all-gather(bf16[4,64,64]{2,1,0:T(8,128)(2,1)S(1)} %copy.184), channel_id=2, replica_groups=mesh['sp'=4,'tp'=8] {'sp'}, dimensions={0}, use_global_device_ids=true | all-gather | bytes 163840 | tf_op jit(solution)/shard_map/all_gather | solution.py:17
  531.0 8.9 all-gather.1
  539.9 5.1 while.65
  568.9 35.6 %while.66 = (s32[]{:T(128)}, f32[4,64,64]{1,2,0:T(8,128)S(1)}, f32[4,64,64]{1,2,0:T(8,128)S(1)}, f32[8,4,64,64]{2,3,1,0:T(8,128)}, f32[8,4,64,64]{2,3,1,0:T(8,12...) while((s32[]{:T(128)}, f32[4,64,64]{1,2,0:T(8,128)S(1)}, ...), condition=%wide.region_8.10_spmd.clone, body=%wide.region_7.9_spmd.clone.sunk | while | flops 25214980 | bytes 1507456 | solution.py:109
  605.3 9.5 all-gather.2
  614.9 8.7 all-gather.3
  623.6 8.5 while.67
  648.0 35.4 %reduce-scatter.3.cloned.1.call-done = bf16[64,2048]{1,0:T(8,128)(2,1)} async-done(((bf16[512,2048]{1,0:T(8,128)(2,1)}), bf16[64,2048]{1,0:T(8,128)(2,1)}) %reduce-scatter.3.cloned.1.call-update) | async-done | bytes 262160 | tf_op jit(solution)/shard_map/reduce_scatter | solution.py:182
  687.4 12.4 %all_to_all.10 = bf16[4,24,2,2048]{3,2,1,0:T(2,128)(2,1)S(1)} all-to-all(bf16[4,24,2,2048]{3,2,1,0:T(2,128)(2,1)} %reshape.265), channel_id=1, replica_groups=mesh['sp'=4,'tp'=8] {'sp'}, dimensions={0} | all-to-all | bytes 1572864 | tf_op jit(solution)/shard_map/all_to_all | solution.py:215
  703.3 81.2 %all-gather.6.cloned.1.call-done = bf16[2048,2048]{1,0:T(8,128)(2,1)} async-done(((bf16[256,2048]{1,0:T(8,128)(2,1)}), bf16[2048,2048]{1,0:T(8,128)(2,1)}) %all-gather.6.cloned.1.call-update) | async-done | bytes 8388624 | tf_op jit(solution)/shard_map/all_gather | solution.py:218
  787.7 6.6 slice.55
  794.3 11.2 %reshape.268 = bf16[768,2,2048]{2,1,0:T(2,128)(2,1)} reshape(bf16[8,192,2048]{2,1,0:T(8,128)(2,1)} %slice.55) | data formatting | bytes 12582912 | tf_op jit(solution)/shard_map/reshape | solution.py:221
  805.5 9.3 fusion.42
  814.9 16.5 %convert_bitcast_fusion = bf16[768,2,2048]{2,0,1:T(8,128)(2,1)} fusion(bf16[2,512,2048]{2,1,0:T(8,128)(2,1)} %param.42, f32[2,768,512]{2,1,0:T(8,128)} %fusion.42, bf16[2,2048,512]{2,1,0:T(8,128)(2,1)} %param.41, bf16[768,2,2048]{2,1,0:T(2,128)(2,1)} %reshape.268), kind=kOutput, calls=%fused_computation.55 | convolution fusion | flops 6450315264 | bytes 24117248 | tf_op jit(solution)/shard_map/rjh,jhd->rjd/dot_general | solution.py:229
  831.4 12.6 %copy.229 = bf16[768,2,2048]{2,1,0:T(2,128)(2,1)} copy(bf16[768,2,2048]{2,0,1:T(8,128)(2,1)} %convert_bitcast_fusion) | data formatting | bytes 12582912 | tf_op jit(solution)/shard_map/rjh,jhd->rjd/transpose | solution.py:229
  844.0 10.3 %reshape.269 = bf16[8,192,2048]{2,1,0:T(8,128)(2,1)} reshape(bf16[768,2,2048]{2,1,0:T(2,128)(2,1)} %copy.229) | data formatting | bytes 12582912 | tf_op jit(solution)/shard_map/reshape | solution.py:232
  858.8 6.2 convolution_convert_fusion.1
  865.0 8.4 pad_maximum_fusion
  873.4 88.1 %reduce-scatter.5.cloned.1.call-done = bf16[256,2048]{1,0:T(8,128)(2,1)} async-done(((bf16[2048,2048]{1,0:T(8,128)(2,1)}), bf16[256,2048]{1,0:T(8,128)(2,1)}) %reduce-scatter.5.cloned.1.call-update) | async-done | bytes 1048592 | tf_op jit(solution)/shard_map/reduce_scatter | solution.py:240
  968.4 8.5 all-to-all-done.1
  (404 shorter events, 302.3 us)
Async XLA Ops:
  6.5 852.2 %copy-start = (bf16[512,2048]{1,0:T(8,128)(2,1)S(1)}, bf16[512,2048]{1,0:T(8,128)(2,1)}, u32[]{:S(2)}) copy-start(bf16[512,2048]{1,0:T(8,128)(2,1)} %param.45) | copy-start | bytes 6291460
  6.5 676.9 %reduce-scatter.3.cloned.1.call-start = ((), (), s32[]{:S(2)}) async-start(), calls=%async_computation.4 | async-start | bytes 2359296 | tf_op jit(solution)/shard_map/reduce_scatter | solution.py:182
  7.8 6.7 copy-start.51
  9.7 277.6 %copy-start.42 = (f32[64,64]{1,0:T(8,128)}, f32[64,64]{1,0:T(8,128)S(1)}, u32[]{:S(2)}) copy-start(f32[64,64]{1,0:T(8,128)S(1)} %get-tuple-element.531) | copy-start | bytes 49156
  36.5 5.8 copy-start.19
  36.5 5.8 copy-start.29
  233.9 10.0 %copy-start.26 = (f32[512,256]{0,1:T(8,128)S(1)}, f32[512,256]{0,1:T(8,128)}, u32[]{:S(2)}) copy-start(f32[512,256]{0,1:T(8,128)} %copy-done.25) | copy-start | bytes 1572868
  287.3 6.7 copy-start.10
  290.7 7.8 copy-start.45
  473.7 8.0 copy-start.48
  483.9 55.9 %copy-start.27 = (f32[4,64,64]{1,2,0:T(8,128)S(1)}, f32[4,64,64]{1,2,0:T(8,128)}, u32[]{:S(2)}) copy-start(f32[4,64,64]{1,2,0:T(8,128)} %custom-call.5) | copy-start | bytes 196612
  519.3 25.7 %copy-start.24 = (bf16[8,64,4,64]{3,2,1,0:T(4,128)(2,1)S(1)}, bf16[8,64,4,64]{3,2,1,0:T(4,128)(2,1)}, u32[]{:S(2)}) copy-start(bf16[8,64,4,64]{3,2,1,0:T(4,128)(2,1)} %reshape_reshape.8) | copy-start | bytes 786436
  548.5 7.1 copy-start.2
  550.7 8.9 copy-start.44
  555.6 7.7 copy-start.12
  555.6 7.7 copy-start.36
  559.5 7.1 copy-start.49
  604.5 27.6 %copy-start.13 = (f32[8,4,64,64]{3,2,1,0:T(8,128)S(1)}, f32[8,4,64,64]{3,2,1,0:T(8,128)}, u32[]{:S(2)}) copy-start(f32[8,4,64,64]{3,2,1,0:T(8,128)} %copy.203) | copy-start | bytes 1572868
  644.8 38.6 %copy-start.40 = (bf16[64,2048]{1,0:T(8,128)(2,1)S(1)}, bf16[64,2048]{1,0:T(8,128)(2,1)}, u32[]{:S(2)}) copy-start(bf16[64,2048]{1,0:T(8,128)(2,1)} %param.28) | copy-start | bytes 786436
  646.9 137.6 %all-gather.6.cloned.1.call-start = ((), (), s32[]{:S(2)}) async-start(), calls=%async_computation.5 | async-start | bytes 9437184 | tf_op jit(solution)/shard_map/all_gather | solution.py:218
  703.2 258.4 %reduce-scatter.5.cloned.1.call-start = ((), (), s32[]{:S(2)}) async-start(), calls=%async_computation.6 | async-start | bytes 9437184 | tf_op jit(solution)/shard_map/reduce_scatter | solution.py:240
  873.4 94.4 %copy-start.54 = (f32[64,2]{0,1:T(2,128)S(1)}, f32[64,2]{0,1:T(2,128)}, u32[]{:S(2)}) copy-start(f32[64,2]{0,1:T(2,128)} %param.39) | copy-start | bytes 1540
  873.4 104.7 %copy-start.41 = (bf16[64,2048]{1,0:T(8,128)(2,1)S(1)}, bf16[64,2048]{1,0:T(8,128)(2,1)}, u32[]{:S(2)}) copy-start(bf16[64,2048]{1,0:T(8,128)(2,1)} %reduce-scatter.3.cloned.1.call-done) | copy-start | bytes 786436
  964.2 12.7 %all-to-all-start.1 = ((bf16[4,24,2,2048]{3,2,1,0:T(2,128)(2,1)}), bf16[4,24,2,2048]{3,2,1,0:T(2,128)(2,1)S(1)}, u32[]{:S(2)}, u32[]{:S(2)}) async-start(bf16[4,24,2,2048]{3,2,1,0:T(2,128)(2,1)} %reshape.272), calls=%async_computation.3 | async-start | bytes 1572864 | tf_op jit(solution)/shard_map/all_to_all | solution.py:253
  (37 other events, 131.0 us)
Sparse Core Ops, SparseCore 0:
  647.0 36.3 reduce-scatter.2
  703.3 81.1 all-gather.5
  873.5 88.0 reduce-scatter.4
where the time goes:
time: 998 us; the launch traced here: 987 us
  other arithmetic  362 us (36%)
  waiting for transfers between devices  213 us (21%)
  matrix products  179 us (18%)
  local copies, waits for them, and re-layouts  161 us (16%)
  blocking collectives  51 us (5%)
  between operations  14.2 us (1%)
    another operation x4, other arithmetic, block_terms(): jax.scipy.linalg.solve_triangular(triangle, right_side, lower=True, unit_...  318 us
    reduce_scatter x1, waiting for transfers between devices, body(): lax.psum_scatter(jnp.concatenate([routed_out, shared_out], axis=1).reshap...  88.1 us
    all_gather x1, waiting for transfers between devices, body(): everyone = lax.all_gather(own_block, 'tp', axis=0, tiled=True)  81.2 us
    dot_general x40, matrix products, chain_product(): jnp.einsum('...ij,...jk->...ik', left_mat, right_mat, precision=highest)  50.2 us
    all_gather x4, blocking collectives, entering(): lax.all_gather(part.astype(kind), axis)  38.6 us
    reduce_scatter x1, waiting for transfers between devices, body(): lax.psum_scatter(jnp.dot(slab, output_weight, preferred_element_type=jnp....  35.4 us
    dot_general x8, matrix products, pairs(): jnp.einsum('bhtn,bhsn->bhts', left_rows, right_rows, precision=highest)  32.2 us
    reshape x11, local copies, waits for them, and re-layouts, to_blocks(): array.reshape(block_count, span_len, head_number, head_width)  23.9 us
  transfers between devices with their start and end apart: 4, of which 4 were waited for; matrix products, arithmetic and copies ran while one was open for 0% of the time, Pallas kernels for 0%

commit v1 on v0

v1 whole, which is shorter than its diff:
```python
import functools
import jax
import jax.numpy as jnp
from jax import lax
from jax.experimental import pallas as pl
from jax.experimental.pallas import tpu as pltpu
from jax.sharding import PartitionSpec as P

highest = lax.Precision.HIGHEST

GN_EPS = 0.00064
RMS_EPS = 1e-06
LANES = 128
F32, BF16 = jnp.float32, jnp.bfloat16


def split(x):
    high = x.astype(BF16)
    return high, (x - high.astype(F32)).astype(BF16)


def dot(x, y):
    return jnp.dot(x, y, preferred_element_type=F32)


def dot_nt(x, y):
    return lax.dot_general(x, y, (((1,), (1,)), ((), ())), preferred_element_type=F32)


def head_of_lane(shape, head):
    return lax.broadcasted_iota(jnp.int32, shape, len(shape) - 1) // head


def expand(x, head):
    which = head_of_lane(x.shape, head)
    zero = jnp.zeros_like(x)
    return jnp.concatenate([jnp.where(which == h, x, zero) for h in range(x.shape[1] // head)], axis=0)


def wide(y, head):
    high, low = split(y)
    return jnp.concatenate([expand(high, head), expand(low, head)], axis=1)


def tall(x):
    high, low = split(x)
    return jnp.concatenate([high, low], axis=0)


def fold(out, rows, columns=LANES):
    return out[:rows, :columns] + (out[rows:, :columns] + out[:rows, columns:])


def times(x, y, head):
    return fold(dot(tall(x), wide(y, head)), x.shape[0])


def mixer_kernel(head, group, r_ref, k_ref, v_ref, e_ref, d_ref, s_ref,
                 loc_ref, rpf_ref, rpb_ref, maps_ref, ro_ref, pc_ref):
    tokens, width = k_ref.shape
    pairs, span = width // LANES, head
    per = LANES // head
    blocks = tokens // span
    row = lax.broadcasted_iota(jnp.int32, (span, LANES), 0)
    lane = lax.broadcasted_iota(jnp.int32, (span, LANES), 1)
    col = lane % head
    which = lane // head
    eye = (row == col).astype(F32)
    ones_bd = expand(jnp.ones((head, LANES), BF16), head)
    tri_row = lax.broadcasted_iota(jnp.int32, (span, span), 0)
    tri_col = lax.broadcasted_iota(jnp.int32, (span, span), 1)
    tri = (tri_row >= tri_col).astype(BF16)
    tri3 = jnp.concatenate([tri, tri, tri], axis=1)

    def prepare(at, p):
        lanes = slice(p * LANES, (p + 1) * LANES)
        rows = pl.ds(pl.multiple_of(at * span, span), span)
        keys = k_ref[rows, lanes].astype(F32)
        square = keys * keys
        total = dot(tall(square), ones_bd)
        unit = keys * lax.rsqrt(total[:span] + total[span:] + 1e-06)
        beta = unit / (1.0 + jnp.exp(-e_ref[rows, lanes].astype(F32)))
        spike = s_ref[rows, p * per:p * per + 1]
        for h in range(1, per):
            spike = jnp.where(which == h, s_ref[rows, p * per + h:p * per + h + 1], spike)
        log_decay = spike - 0.6065306597126334 / (1.0 + jnp.exp(-d_ref[rows, lanes].astype(F32)))
        high = log_decay.astype(BF16)
        rest = log_decay - high.astype(F32)
        mid = rest.astype(BF16)
        low = (rest - mid.astype(F32)).astype(BF16)
        cum = dot(tri3, jnp.concatenate([high, mid, low], axis=0))
        before = cum - log_decay
        centre, end = cum[span // 2 - 1:span // 2], cum[span - 1:span]
        e1, e0 = jnp.exp(cum - centre), jnp.exp(before - centre)
        i1, i0 = jnp.exp(centre - cum), jnp.exp(centre - before)
        fa, fb, fe = jnp.exp(centre), jnp.exp(end - centre), jnp.exp(end)
        read = r_ref[rows, lanes].astype(F32)
        forward = dict(u=unit * e0, r=read * e1, b=beta * i1, k=keys * i1, start=fa, total=fb)
        backward = dict(u=unit * i1, r=read * i0, b=beta * e0, k=keys * e0, start=fb, total=fa)
        for d, unit_of in ((0, forward), (1, backward)):
            unit_of.update(end=fe, v=v_ref[rows, lanes], at=at, p=p, d=d, lanes=lanes, rows=rows)
        return [forward, backward]

    same = [(row // (8 << i)) == (col // (8 << i)) for i in range(8) if (8 << i) <= span]
    strict = (row > col, row < col)
    incl = (row >= col, row <= col)

    def one_group(i, carry):
        units = []
        for g in range(group):
            for p in range(pairs):
                units += prepare(i * group + g, p)
        for q in units:
            left = tall(jnp.concatenate([q["u"], q["r"], eye * q["total"]], axis=0))
            bh, bl = split(q["b"])
            kh, kl = split(q["k"])
            right = jnp.concatenate([expand(x, head) for x in (bh, bl)], axis=0)
            out = fold(dot_nt(left, right), 3 * span)
            q["ub"] = jnp.where(strict[q["d"]], out[:span], 0.0)
            q["rb"] = jnp.where(incl[q["d"]], out[span:2 * span], 0.0)
            q["be"] = out[2 * span:]
            right = jnp.concatenate([expand(x, head) for x in (kh, kl)], axis=0)
            out = fold(dot_nt(left, right), 3 * span)
            q["uk"] = jnp.where(strict[q["d"]], out[:span], 0.0)
            q["rk"] = jnp.where(incl[q["d"]], out[span:2 * span], 0.0)
            q["ke"] = out[2 * span:]
        for q in units:
            q["D"] = jnp.where(same[0], q["ub"], 0.0)
            q["x"] = eye - q["D"]
        for q in units:
            q["D2"] = times(q["D"], q["D"], head)
        for q in units:
            left = jnp.concatenate([q["x"], q["D2"]], axis=0)
            out = times(left, q["D2"], head)
            q["x"], q["D4"] = q["x"] + out[:span], out[span:]
        for q in units:
            q["x"] = q["x"] + times(q["x"], q["D4"], head)
        for level in range(1, len(same)):
            for q in units:
                off = jnp.where(same[level] & ~same[level - 1], q["ub"], 0.0)
                q["t"] = times(q["x"], off, head)
            for q in units:
                q["x"] = q["x"] - times(q["t"], q["x"], head)
        for q in units:
            left = tall(jnp.concatenate([q["uk"], q["rk"], q["ke"]], axis=0))
            out = dot(left, expand(q["v"], head))
            out = out[:3 * span] + out[3 * span:]
            q["ukv"], q["rkv"], q["kev"] = out[:span], out[span:2 * span], out[2 * span:]
        for q in units:
            left = tall(q["x"])
            q["w"] = fold(dot(left, wide(q["u"] * q["start"], head)), span)
            q["y"] = fold(dot(left, wide(-q["ukv"], head)), span)
        for q in units:
            left = tall(jnp.concatenate([q["rb"], q["be"]], axis=0))
            ow = fold(dot(left, wide(q["w"], head)), 2 * span)
            oy = fold(dot(left, wide(q["y"], head)), 2 * span)
            readout = q["r"] * q["start"] - ow[:span]
            local = oy[:span] + q["rkv"]
            step = eye * q["end"] - ow[span:]
            carried = oy[span:] + q["kev"]
            at = (q["d"] * pairs + q["p"]) * blocks + q["at"]
            ro_ref[at, :span] = step
            ro_ref[at, span:] = readout
            pc_ref[at] = carried
            if q["d"] == 0:
                q_first = local
            else:
                loc_ref[q["rows"], q["lanes"]] = q_first + local
        return carry

    lax.fori_loop(0, blocks // group, one_group, 0)

    start = tuple(
        (jnp.zeros((span, LANES), F32), eye) for _ in range(2 * pairs)
    )

    def advance(i, states):
        after = []
        for c, (state, product) in enumerate(states):
            d, p = c // pairs, c % pairs
            at = i if d == 0 else blocks - 1 - i
            lanes = slice(p * LANES, (p + 1) * LANES)
            rows = pl.ds(pl.multiple_of(at * span, span), span)
            left = tall(ro_ref[c * blocks + at])
            zs = fold(dot(left, wide(state, head)), 2 * span)
            ps = fold(dot(left, wide(product, head)), 2 * span)
            loc_ref[rows, lanes] += zs[span:]
            (rpf_ref, rpb_ref)[d][rows, lanes] = ps[span:]
            after.append((zs[:span] + pc_ref[c * blocks + at], ps[:span]))
        return tuple(after)

    states = lax.fori_loop(0, blocks, advance, start)
    for c, (state, product) in enumerate(states):
        maps_ref[c, 0] = state.astype(BF16)
        maps_ref[c, 1] = product.astype(BF16)


def finish_kernel(head, count, place_ref, maps_ref, loc_ref, rpf_ref, rpb_ref, gain_ref, out_ref):
    tokens, width = loc_ref.shape
    pairs = width // LANES
    place = place_ref[0]
    entries = []
    for c in range(2 * pairs):
        state = jnp.zeros((head, LANES), F32)
        for far in range(count - 1, 0, -1):
            s = far if c < pairs else count - far
            reached = (place >= far) if c < pairs else (place + far < count)
            out = dot(maps_ref[s - 1, c, 1], wide(state, head))
            new = out[:, :LANES] + out[:, LANES:] + maps_ref[s - 1, c, 0].astype(F32)
            state = jnp.where(reached, new, state)
        entries.append(state)
    mean_bd = expand(jnp.full((head, LANES), 1.0 / head, BF16), head)
    for p in range(pairs):
        lanes = slice(p * LANES, (p + 1) * LANES)
        mix = (
            loc_ref[:, lanes]
            + times(rpf_ref[:, lanes], entries[p], head)
            + times(rpb_ref[:, lanes], entries[pairs + p], head)
        )
        total = dot(tall(mix), mean_bd)
        away = mix - (total[:tokens] + total[tokens:])
        total = dot(tall(away * away), mean_bd)
        scaled = away * lax.rsqrt(total[:tokens] + total[tokens:] + GN_EPS)
        out_ref[:, lanes] = (scaled * gain_ref[:, lanes].astype(F32)).astype(BF16)


def vmem_call(kernel, out_shape, scratch=(), scalars=0, flops=0, limit=48 << 20):
    many = isinstance(out_shape, (tuple, list))
    return lambda *args: pl.pallas_call(
        kernel,
        out_shape=out_shape,
        in_specs=[pl.BlockSpec(memory_space=pltpu.SMEM)] * scalars
        + [pl.BlockSpec(memory_space=pltpu.VMEM)] * (len(args) - scalars),
        out_specs=jax.tree.map(lambda _: pl.BlockSpec(memory_space=pltpu.VMEM), out_shape),
        scratch_shapes=list(scratch),
        compiler_params=pltpu.CompilerParams(vmem_limit_bytes=limit),
        cost_estimate=pl.CostEstimate(flops=flops, bytes_accessed=4 << 20, transcendentals=0),
    )(*args)


def mixer(receptance, keys, values, erase_preact, decay_preact, decay_spike, head_norm_gain):
    tokens, width = keys.shape
    head = width // decay_spike.shape[1]
    pairs, blocks = width // LANES, tokens // head
    count, place = lax.axis_size("sp"), lax.axis_index("sp")
    shape = jax.ShapeDtypeStruct((tokens, width), F32)
    group = 2 if blocks % 2 == 0 else 1
    local, read_f, read_b, maps = vmem_call(
        functools.partial(mixer_kernel, head, group),
        (shape, shape, shape, jax.ShapeDtypeStruct((2 * pairs, 2, head, LANES), BF16)),
        [
            pltpu.VMEM((2 * pairs * blocks, 2 * head, LANES), F32),
            pltpu.VMEM((2 * pairs * blocks, head, LANES), F32),
        ],
        flops=20_000_000_000,
    )(receptance, keys, values, erase_preact, decay_preact, decay_spike)
    arrived = [
        lax.ppermute(maps, "sp", [(i, (i + s) % count) for i in range(count)])
        for s in range(1, count)
    ]
    return vmem_call(
        functools.partial(finish_kernel, head, count),
        jax.ShapeDtypeStruct((tokens, width), BF16),
        scalars=1,
        flops=4_000_000_000,
    )(
        place.astype(jnp.int32).reshape(1),
        jnp.stack(arrived),
        local, read_f, read_b,
        head_norm_gain.reshape(1, width),
    )


def body(
    layer_input,
    receptance,
    keys,
    values,
    erase_preact,
    decay_preact,
    decay_spike,
    head_norm_gain,
    output_weight,
    expert_norm_gain,
    routes,
    routing_weight,
    expert_gate_weight,
    expert_up_weight,
    expert_down_weight,
    shared_gate_weight,
    shared_up_weight,
    shared_down_weight,
):
    mixed = mixer(
        receptance, keys, values, erase_preact, decay_preact, decay_spike, head_norm_gain
    )
    row_count = layer_input.shape[0]
    model_width = layer_input.shape[1]
    slab = mixed
    projected = lax.psum_scatter(
        jnp.dot(slab, output_weight, preferred_element_type=jnp.float32).astype(jnp.bfloat16),
        "tp",
        scatter_dimension=0,
        tiled=True,
    ).astype(jnp.float32)
    residual = layer_input.astype(jnp.float32) + projected
    normed = residual * lax.rsqrt(jnp.mean(residual * residual, axis=-1, keepdims=True) + RMS_EPS)
    normed = (normed * expert_norm_gain.astype(jnp.float32)).astype(jnp.bfloat16)
    top_count = routes.shape[1]
    expert_local = expert_gate_weight.shape[0]
    sp_count = lax.axis_size("sp")
    expert_total = expert_local * sp_count
    capacity = max(2, (3 * row_count * top_count + 2 * expert_total - 1) // (2 * expert_total))
    slot_total = sp_count * capacity * expert_local
    entries = routes.reshape(-1)
    entry_count = entries.shape[0]
    expert_hot = (entries[:, None] == lax.broadcasted_iota(jnp.int32, (1, expert_total), 1)).astype(
        jnp.int32
    )
    rank_in = jnp.sum((jnp.cumsum(expert_hot, axis=0) - 1) * expert_hot, axis=1)
    slot_of = (entries // expert_local * capacity + rank_in) * expert_local + entries % expert_local
    slot_hot = (slot_of[:, None] == lax.broadcasted_iota(jnp.int32, (1, slot_total), 1)).astype(
        jnp.float32
    )
    owner_hot = (
        lax.broadcasted_iota(jnp.int32, (entry_count, 1), 0) // top_count
        == lax.broadcasted_iota(jnp.int32, (1, row_count), 1)
    ).astype(jnp.float32)
    placing = jnp.dot(slot_hot.T, owner_hot, precision=highest)
    weighting = jnp.dot(owner_hot.T, slot_hot * routing_weight.reshape(-1, 1), precision=highest)
    outgoing = jnp.dot(placing.astype(jnp.bfloat16), normed, preferred_element_type=jnp.float32)
    outgoing = outgoing.astype(jnp.bfloat16).reshape(sp_count, capacity, expert_local, model_width)
    arrived = lax.all_to_all(outgoing, "sp", split_axis=0, concat_axis=0, tiled=True)
    own_block = jnp.concatenate([arrived.reshape(slot_total, model_width), normed], axis=0)
    block_rows = own_block.shape[0]
    everyone = lax.all_gather(own_block, "tp", axis=0, tiled=True)
    slab = everyone
    slab = slab.reshape(block_rows * lax.axis_size("tp") // block_rows, block_rows, model_width)
    routed_in = slab[:, :slot_total].reshape(-1, expert_local, model_width)
    gate_value = jnp.einsum(
        "rjd,jdh->rjh", routed_in, expert_gate_weight, preferred_element_type=jnp.float32
    )
    up_value = jnp.einsum(
        "rjd,jdh->rjh", routed_in, expert_up_weight, preferred_element_type=jnp.float32
    )
    hidden = (jax.nn.silu(gate_value) * up_value).astype(jnp.bfloat16)
    routed_out = jnp.einsum(
        "rjh,jhd->rjd", hidden, expert_down_weight, preferred_element_type=jnp.float32
    )
    routed_out = routed_out.reshape(-1, slot_total, model_width)
    shared_in = slab[:, slot_total:].reshape(-1, model_width)
    shared_hidden = (
        jax.nn.silu(jnp.dot(shared_in, shared_gate_weight, preferred_element_type=jnp.float32))
        * jnp.dot(shared_in, shared_up_weight, preferred_element_type=jnp.float32)
    ).astype(jnp.bfloat16)
    shared_out = jnp.dot(shared_hidden, shared_down_weight, preferred_element_type=jnp.float32)
    shared_out = shared_out.reshape(-1, row_count, model_width)
    summed = lax.psum_scatter(
        jnp.concatenate([routed_out, shared_out], axis=1)
        .reshape(block_rows * lax.axis_size("tp"), model_width)
        .astype(jnp.bfloat16),
        "tp",
        scatter_dimension=0,
        tiled=True,
    ).astype(jnp.float32)
    routed_rows = (
        summed[:slot_total]
        .astype(jnp.bfloat16)
        .reshape(sp_count, capacity, expert_local, model_width)
    )
    returned = lax.all_to_all(routed_rows, "sp", split_axis=0, concat_axis=0, tiled=True)
    routed = jnp.dot(
        weighting, returned.reshape(slot_total, model_width).astype(jnp.float32), precision=highest
    )
    return (residual + summed[slot_total:] + routed).astype(jnp.bfloat16)


def solution(mesh):
    return jax.shard_map(
        body,
        mesh=mesh,
        in_specs=(
            P(("sp", "tp"), None),
            P("sp", "tp"),
            P("sp", "tp"),
            P("sp", "tp"),
            P("sp", "tp"),
            P("sp", "tp"),
            P("sp", "tp"),
            P("tp"),
            P("tp", None),
            P(),
            P(("sp", "tp"), None),
            P(("sp", "tp"), None),
            P("sp", None, "tp"),
            P("sp", None, "tp"),
            P("sp", "tp", None),
            P(None, "tp"),
            P(None, "tp"),
            P("tp", None),
        ),
        out_specs=P(("sp", "tp"), None),
        check_vma=False,
    )
```

time: 998 us -> 390 us (0.39)
  other arithmetic: 362 us -> 14.2 us
  matrix products: 179 us -> 41.9 us
  local copies, waits for them, and re-layouts: 161 us -> 57.9 us
  blocking collectives: 51 us -> 12.4 us
  Pallas kernels: 0 us -> 20.9 us
    another operation x6 -> x1, other arithmetic: 320 us -> 0.95 us  [mixer(): jnp.stack(arrived)]
    dot_general x66 -> x0, matrix products: 132 us -> none  [the longest x40 50.2 us: chain_product(): jnp.einsum('...ij,...jk->...ik', left_mat, right_mat, precision=highest)]
    all_gather x4 -> x0, blocking collectives: 38.6 us -> none  [entering(): lax.all_gather(part.astype(kind), axis)]
    reshape x15 -> x1, local copies, waits for them, and re-layouts: 31.1 us -> 0.01 us  [mixer(): head_norm_gain.reshape(1, width)]
    pallas_call x0 -> x2, Pallas kernels: none -> 20.9 us  [vmem_call(): pl.pallas_call(kernel, out_shape=out_shape, in_specs=[pl.BlockSpec(memory...]
    dynamic_slice x48 -> x0, local copies, waits for them, and re-layouts: 20.5 us -> none  [the longest x32 16.2 us: block_chain(): lax.scan(advance, (identity, jnp.zeros_like(identity)), (transition, carr...]
    rev x7 -> x0, local copies, waits for them, and re-layouts: 17.9 us -> none  [the longest x6 15.7 us: body(): array[::-1]]
    dynamic_update_slice x16 -> x0, other arithmetic: 11.9 us -> none  [block_chain(): lax.scan(advance, (identity, jnp.zeros_like(identity)), (transition, carr...]
  transfers between devices with their start and end apart: 4 -> 7, of which waited for: 4 -> 6; matrix products, arithmetic and copies ran while one was open for 0% -> 0% of each run, Pallas kernels for 0% -> 0%
where the time goes in v1:
time: 390 us; the launch traced here: 388 us
  waiting for transfers between devices  219 us (56%)
  local copies, waits for them, and re-layouts  57.9 us (15%)
  matrix products  41.9 us (11%)
  Pallas kernels  20.9 us (5%)
  other arithmetic  14.2 us (4%)
  between operations  13.3 us (3%)
  blocking collectives  12.4 us (3%)
  starting transfers between devices  8.93 us (2%)
    reduce_scatter x1, waiting for transfers between devices, body(): lax.psum_scatter(jnp.concatenate([routed_out, shared_out], axis=1).reshap...  88.1 us
    all_gather x1, waiting for transfers between devices, body(): everyone = lax.all_gather(own_block, 'tp', axis=0, tiled=True)  81.1 us
    reduce_scatter x1, waiting for transfers between devices, body(): lax.psum_scatter(jnp.dot(slab, output_weight, preferred_element_type=jnp....  34.4 us
    pallas_call x2, Pallas kernels, vmem_call(): pl.pallas_call(kernel, out_shape=out_shape, in_specs=[pl.BlockSpec(memory...  20.9 us
    dot_general x1, matrix products, body(): jnp.einsum('rjh,jhd->rjd', hidden, expert_down_weight, preferred_element_...  16.5 us
    transpose x1, local copies, waits for them, and re-layouts, body(): jnp.einsum('rjh,jhd->rjd', hidden, expert_down_weight, preferred_element_...  12.7 us
    all_to_all x1, blocking collectives, body(): lax.all_to_all(outgoing, 'sp', split_axis=0, concat_axis=0, tiled=True)  12.4 us
    reshape x1, local copies, waits for them, and re-layouts, body(): routed_in = slab[:, :slot_total].reshape(-1, expert_local, model_width)  10.9 us
  transfers between devices with their start and end apart: 7, of which 6 were waited for; matrix products, arithmetic and copies ran while one was open for 0% of the time, Pallas kernels for 0%

profile of v1, /device:TPU:0, one launch (start us, length us, event | category | flops | bytes accessed | tf_op | source)
XLA Modules:
  0.0 388.5 jit_solution(8140543384222627400)
XLA Ops:
  12.3 18.7 %shard_map.172 = (f32[512,256]{1,0:T(8,128)S(1)}, f32[512,256]{1,0:T(8,128)S(1)}, f32[512,256]{1,0:T(8,128)S(1)}, bf16[4,2,64,128]{3,2,1,0:T(8,128)(2,1)S(1)}) custom-call(bf16[512,256]{1,0:T(8,128)(2,1)S(1)} %copy-done.1, bf16[512,256]{1,0:T(8,128)(2,1)S(1)} %copy-done.2, bf16[512,256]{1,0:T(8,128)(2,1)S(1)} %copy-done.3, bf16[512,256]{1,0:T(8,128)(2,1)S(1)} %copy-done.4, ...), custom_call_target="tpu_custom_call" | custom-call | flops 20000000000 | bytes 4194304 | tf_op jit(solution)/shard_map/pallas_call | solution.py:229
  31.8 3.9 %collective-permute-start.2 = (bf16[4,2,64,128]{3,2,1,0:T(8,128)(2,1)S(1)}, bf16[4,2,64,128]{3,2,1,0:T(8,128)(2,1)S(1)}, u32[]{:S(2)}, u32[]{:S(2)}) collective-permute-start(bf16[4,2,64,128]{3,2,1,0:T(8,128)(2,1)S(1)} %get-tuple-element.9), channel_id=1, source_target_pairs={{0,24},{8,0},{16,8},{24,16},{1,25},{9,1},{17,9},{25,17},{2,26},{10... | collective-permute-start | bytes 393224 | tf_op jit(solution)/shard_map/ppermute | solution.py:258
  36.8 2.8 collective-permute-done.2
  39.6 3.9 collective-permute-done.1
  45.4 2.2 shard_map.173
  47.7 2.1 convolution_convert_fusion
  50.9 34.4 %reduce-scatter.3.cloned.1.call-done = bf16[64,2048]{1,0:T(8,128)(2,1)} async-done(((bf16[512,2048]{1,0:T(8,128)(2,1)}), bf16[64,2048]{1,0:T(8,128)(2,1)}) %reduce-scatter.3.cloned.1.call-update) | async-done | bytes 262160 | tf_op jit(solution)/shard_map/reduce_scatter | solution.py:300
  89.2 12.4 %all_to_all.10 = bf16[4,24,2,2048]{3,2,1,0:T(2,128)(2,1)S(1)} all-to-all(bf16[4,24,2,2048]{3,2,1,0:T(2,128)(2,1)} %reshape.146), channel_id=1, replica_groups=mesh['sp'=4,'tp'=8] {'sp'}, dimensions={0} | all-to-all | bytes 1572864 | tf_op jit(solution)/shard_map/all_to_all | solution.py:333
  102.8 2.3 pad_maximum_fusion.1
  105.4 81.1 %all-gather.2.cloned.1.call-done = bf16[2048,2048]{1,0:T(8,128)(2,1)} async-done(((bf16[256,2048]{1,0:T(8,128)(2,1)}), bf16[2048,2048]{1,0:T(8,128)(2,1)}) %all-gather.2.cloned.1.call-update) | async-done | bytes 8388624 | tf_op jit(solution)/shard_map/all_gather | solution.py:336
  186.5 3.2 slice.22
  189.7 6.6 %slice.21 = bf16[8,192,2048]{2,1,0:T(8,128)(2,1)} slice(bf16[8,256,2048]{2,1,0:T(8,128)(2,1)} %bitcast.47), slice={[0:8], [0:192], [0:2048]} | slice | bytes 12582912 | tf_op jit(solution)/shard_map/slice | solution.py:339
  196.3 10.9 %reshape.149 = bf16[768,2,2048]{2,1,0:T(2,128)(2,1)} reshape(bf16[8,192,2048]{2,1,0:T(8,128)(2,1)} %slice.21) | data formatting | bytes 12582912 | tf_op jit(solution)/shard_map/reshape | solution.py:339
  207.1 9.3 %fusion.2 = f32[2,768,512]{2,1,0:T(8,128)} fusion(bf16[2,2048,512]{2,1,0:T(8,128)(2,1)} %param.30, bf16[768,2,2048]{2,1,0:T(2,128)(2,1)} %reshape.149), kind=kOutput, calls=%fused_computation.4 | convolution fusion | flops 3221225472 | bytes 13631488 | tf_op jit(solution)/shard_map/rjd,jdh->rjh/dot_general | solution.py:340
  216.5 16.5 %convert_bitcast_fusion = bf16[768,2,2048]{2,0,1:T(8,128)(2,1)} fusion(bf16[2,512,2048]{2,1,0:T(8,128)(2,1)} %param.32, f32[2,768,512]{2,1,0:T(8,128)} %fusion.2, bf16[2,2048,512]{2,1,0:T(8,128)(2,1)} %param.31, bf16[768,2,2048]{2,1,0:T(2,128)(2,1)} %reshape.149), kind=kOutput, calls=%fused_computation.1 | convolution fusion | flops 6450315264 | bytes 24117248 | tf_op jit(solution)/shard_map/rjh,jhd->rjd/dot_general | solution.py:347
  232.9 12.7 %copy.25 = bf16[768,2,2048]{2,1,0:T(2,128)(2,1)} copy(bf16[768,2,2048]{2,0,1:T(8,128)(2,1)} %convert_bitcast_fusion) | data formatting | bytes 12582912 | tf_op jit(solution)/shard_map/rjh,jhd->rjd/transpose | solution.py:347
  245.6 10.1 %reshape.150 = bf16[8,192,2048]{2,1,0:T(8,128)(2,1)} reshape(bf16[768,2,2048]{2,1,0:T(2,128)(2,1)} %copy.25) | data formatting | bytes 12582912 | tf_op jit(solution)/shard_map/reshape | solution.py:350
  255.7 4.5 %fusion.29 = f32[512,512]{1,0:T(8,128)} fusion(bf16[512,2048]{1,0:T(8,128)(2,1)} %bitcast.48, bf16[2048,512]{1,0:T(8,128)(2,1)} %param.33), kind=kOutput, calls=%fused_computation.55 | convolution fusion | flops 1073741824 | bytes 5242880 | tf_op jit(solution)/shard_map/dot_general | solution.py:353
  260.2 6.2 %convolution_convert_fusion.1 = bf16[512,2048]{1,0:T(8,128)(2,1)} fusion(bf16[512,2048]{1,0:T(8,128)(2,1)S(1)} %copy-done, bf16[512,2048]{1,0:T(8,128)(2,1)} %bitcast.49, bf16[2048,512]{1,0:T(8,128)(2,1)} %param.34, f32[512,512]{1,0:T(8,128)} %fusion.29), kind=kOutput, calls=%fused_computation.14 | convolution fusion | flops 2150105088 | bytes 9437184 | tf_op jit(solution)/shard_map/dot_general | solution.py:356
  266.4 8.3 %pad_maximum_fusion = bf16[8,256,2048]{2,1,0:T(8,128)(2,1)} fusion(bf16[8,64,2048]{2,1,0:T(8,128)(2,1)} %bitcast.50, bf16[8,192,2048]{2,1,0:T(8,128)(2,1)} %reshape.150), kind=kLoop, calls=%fused_computation | loop fusion | flops 16777216 | bytes 16777216 | tf_op jit(solution)/shard_map/concatenate | solution.py:359
  274.8 88.1 %reduce-scatter.5.cloned.1.call-done = bf16[256,2048]{1,0:T(8,128)(2,1)} async-done(((bf16[2048,2048]{1,0:T(8,128)(2,1)}), bf16[256,2048]{1,0:T(8,128)(2,1)}) %reduce-scatter.5.cloned.1.call-update) | async-done | bytes 1048592 | tf_op jit(solution)/shard_map/reduce_scatter | solution.py:358
  365.5 3.7 all-to-all-start.1
  369.7 8.6 %all-to-all-done.1 = bf16[4,24,2,2048]{3,2,1,0:T(2,128)(2,1)S(1)} async-done(((bf16[4,24,2,2048]{3,2,1,0:T(2,128)(2,1)}), bf16[4,24,2,2048]{3,2,1,0:T(2,128)(2,1)S(1)}, u32[]{:S(2)}, u32[]{:S(2)}) %all-to-all-start.1) | async-done | bytes 786464 | tf_op jit(solution)/shard_map/all_to_all | solution.py:371
  379.5 2.4 fusion.8
  (62 shorter events, 20.4 us)
Async XLA Ops:
  6.5 253.7 %copy-start = (bf16[512,2048]{1,0:T(8,128)(2,1)S(1)}, bf16[512,2048]{1,0:T(8,128)(2,1)}, u32[]{:S(2)}) copy-start(bf16[512,2048]{1,0:T(8,128)(2,1)} %param.35) | copy-start | bytes 6291460
  6.5 78.7 %reduce-scatter.3.cloned.1.call-start = ((), (), s32[]{:S(2)}) async-start(), calls=%async_computation.4 | async-start | bytes 2359296 | tf_op jit(solution)/shard_map/reduce_scatter | solution.py:300
  7.5 1.0 copy-start.1
  8.5 0.9 copy-start.2
  9.4 0.9 copy-start.3
  10.4 0.9 copy-start.4
  11.3 0.9 copy-start.5
  12.3 24.5 %copy-start.14 = (bf16[256]{0:T(256)(128)(2,1)S(1)}, bf16[256]{0:T(256)(128)(2,1)}, u32[]{:S(2)}) copy-start(bf16[256]{0:T(256)(128)(2,1)} %param.25) | copy-start | bytes 1540
  31.0 0.8 copy-start.6
  31.8 7.8 %collective-permute-start.2 = (bf16[4,2,64,128]{3,2,1,0:T(8,128)(2,1)S(1)}, bf16[4,2,64,128]{3,2,1,0:T(8,128)(2,1)S(1)}, u32[]{:S(2)}, u32[]{:S(2)}) collective-permute-start(bf16[4,2,64,128]{3,2,1,0:T(8,128)(2,1)S(1)} %get-tuple-element.9), channel_id=1, source_target_pairs={{0,24},{8,0},{16,8},{24,16},{1,25},{9,1},{17,9},{25,17},{2,26},{10... | collective-permute-start | bytes 393224 | tf_op jit(solution)/shard_map/ppermute | solution.py:258
  35.7 7.8 %collective-permute-start.1 = (bf16[4,2,64,128]{3,2,1,0:T(8,128)(2,1)S(1)}, bf16[4,2,64,128]{3,2,1,0:T(8,128)(2,1)S(1)}, u32[]{:S(2)}, u32[]{:S(2)}) collective-permute-start(bf16[4,2,64,128]{3,2,1,0:T(8,128)(2,1)S(1)} %get-tuple-element.9), channel_id=1, source_target_pairs={{0,16},{8,24},{16,0},{24,8},{1,17},{9,25},{17,1},{25,9},{2,18},{10... | collective-permute-start | bytes 393224 | tf_op jit(solution)/shard_map/ppermute | solution.py:258
  36.2 7.3 %collective-permute-start = (bf16[4,2,64,128]{3,2,1,0:T(8,128)(2,1)S(1)}, bf16[4,2,64,128]{3,2,1,0:T(8,128)(2,1)}, u32[]{:S(2)}, u32[]{:S(2)}) collective-permute-start(bf16[4,2,64,128]{3,2,1,0:T(8,128)(2,1)S(1)} %get-tuple-element.9), channel_id=1, source_target_pairs={{0,8},{8,16},{16,24},{24,0},{1,9},{9,17},{17,25},{25,1},{2,10},{10... | collective-permute-start | bytes 393224 | tf_op jit(solution)/shard_map/ppermute | solution.py:258
  44.4 1.0 copy-start.7
  45.4 2.2 copy-start.10
  47.7 2.2 copy-start.11
  47.7 2.2 copy-start.12
  47.7 37.5 %copy-start.8 = (bf16[64,2048]{1,0:T(8,128)(2,1)S(1)}, bf16[64,2048]{1,0:T(8,128)(2,1)}, u32[]{:S(2)}) copy-start(bf16[64,2048]{1,0:T(8,128)(2,1)} %param.18) | copy-start | bytes 786436
  49.8 136.7 %all-gather.2.cloned.1.call-start = ((), (), s32[]{:S(2)}) async-start(), calls=%async_computation.5 | async-start | bytes 9437184 | tf_op jit(solution)/shard_map/all_gather | solution.py:336
  105.1 257.8 %reduce-scatter.5.cloned.1.call-start = ((), (), s32[]{:S(2)}) async-start(), calls=%async_computation.6 | async-start | bytes 9437184 | tf_op jit(solution)/shard_map/reduce_scatter | solution.py:358
  274.8 94.4 %copy-start.13 = (f32[64,2]{0,1:T(2,128)S(1)}, f32[64,2]{0,1:T(2,128)}, u32[]{:S(2)}) copy-start(f32[64,2]{0,1:T(2,128)} %param.29) | copy-start | bytes 1540
  274.8 104.7 %copy-start.9 = (bf16[64,2048]{1,0:T(8,128)(2,1)S(1)}, bf16[64,2048]{1,0:T(8,128)(2,1)}, u32[]{:S(2)}) copy-start(bf16[64,2048]{1,0:T(8,128)(2,1)} %reduce-scatter.3.cloned.1.call-done) | copy-start | bytes 786436
  365.5 12.8 %all-to-all-start.1 = ((bf16[4,24,2,2048]{3,2,1,0:T(2,128)(2,1)}), bf16[4,24,2,2048]{3,2,1,0:T(2,128)(2,1)S(1)}, u32[]{:S(2)}, u32[]{:S(2)}) async-start(bf16[4,24,2,2048]{3,2,1,0:T(2,128)(2,1)} %reshape.153), calls=%async_computation.3 | async-start | bytes 1572864 | tf_op jit(solution)/shard_map/all_to_all | solution.py:371
Sparse Core Ops, SparseCore 0:
  49.9 35.2 reduce-scatter.2
  105.3 81.2 all-gather.1
  274.9 88.0 reduce-scatter.4
